TPU v7x, 32 devices: a whole 2x2x4 slice. The times are simulated.
32 devices in a mesh: kv: 8 (over z, y), tp: 4 (over x, core).
Axes of the slice: x: 2, y: 2, z: 4, core: 2. Of those that a mesh axis runs over, the one named last changes fastest.
Arguments:
- tokens: bfloat16 [8, 2048], P(None, 'kv'), may hold values from -6 to 6
- in_gain: float32 [2048], P('kv'), may hold values from 0.1 to 1.9
- w_query: bfloat16 [2048, 512], P('kv', 'tp'), may hold values from -0.125 to 0.125
- score_bias: float32 [4], P('tp'), as said below
- cache_keys: bfloat16 [8, 8192, 512], P(None, 'kv', 'tp'), may hold values from -8 to 8, as said below
- cache_values: bfloat16 [8, 8192, 512], P(None, 'kv', 'tp'), may hold values from -6 to 6
- lengths: int32 [8], replicated, may hold values from 1024 to 8192, as said below
- head_gain: float32 [512], P('tp'), may hold values from 0.1 to 1.9
- w_out: bfloat16 [512, 2048], P('tp', 'kv'), may hold values from -0.25 to 0.25
Outputs:
- mixed: bfloat16 [8, 2048], P(None, 'kv')
Inputs may be any that keep to these rules, and one draw needn't show every extreme that they name: `score_bias`: one value a head, added to every score of that head. `cache_keys`: real-valued key entries. `lengths`: one sequence has all 8192 positions cached.
All inputs are finite; a program needn't handle non-finite values.
Results may differ from a plain program's by a relative error of at most 0.0095.
The roundings to bfloat16 on the way count: a program that leaves them out, or rounds other values in their place, can miss the bound.
Values may be sent and summed in bfloat16 or wider, within the bound.
A program may use at most 64 MiB of HBM per device.

v0:
```python
import jax
import jax.numpy as jnp
from jax import lax
from jax.sharding import PartitionSpec as P

D = 2048


EPS = 1e-06


def shards(
    tokens, in_gain, w_query, score_bias, cache_keys, cache_values, lengths, head_gain, w_out
):
    sequences = tokens.shape[0]
    local_len = cache_keys.shape[1]
    head_width = cache_keys.shape[2]
    heads_here = score_bias.shape[0]
    head_size = head_width // heads_here
    as_float = tokens.astype(jnp.float32)
    gained = (as_float * in_gain).astype(jnp.bfloat16)
    partial_value = jnp.dot(gained, w_query, preferred_element_type=jnp.float32)
    squares = jnp.sum(as_float * as_float, axis=1)
    summed, total_sq = lax.psum((partial_value, squares), "kv")
    row_scale = lax.rsqrt(total_sq / D + EPS)
    queries = (
        (summed * row_scale[:, None]).astype(jnp.bfloat16).reshape(sequences, heads_here, head_size)
    )
    key_heads = cache_keys.reshape(sequences, local_len, heads_here, head_size)
    value_heads = cache_values.reshape(sequences, local_len, heads_here, head_size)
    scores = jnp.einsum("bhd,bphd->bhp", queries, key_heads, preferred_element_type=jnp.float32)
    scores = scores * head_size ** (-0.5) + score_bias[None, :, None]
    offset = lax.axis_index("kv") * local_len
    places = offset + lax.iota(jnp.int32, local_len)
    usable = places[None, None, :] < lengths[:, None, None]
    log_keep = jnp.where(usable, jax.nn.log_sigmoid(-scores), 0.0)
    strict_upper = (
        lax.iota(jnp.int32, local_len)[:, None] > lax.iota(jnp.int32, local_len)[None, :]
    ).astype(jnp.float32)
    suffix = jnp.einsum("bhr,rs->bhs", log_keep, strict_upper, precision=lax.Precision.HIGHEST)
    weights = jnp.where(usable, jnp.exp(jax.nn.log_sigmoid(scores) + suffix), 0.0).astype(
        jnp.bfloat16
    )
    local_out = jnp.einsum(
        "bhp,bphd->bhd", weights, value_heads, preferred_element_type=jnp.float32
    )
    seg_total = jnp.sum(log_keep, axis=2)
    every_total = lax.all_gather(seg_total[None], "kv", axis=0, tiled=True)
    ranks_kv = lax.iota(jnp.int32, every_total.shape[0])
    later_sum = jnp.sum(
        jnp.where((ranks_kv > lax.axis_index("kv"))[:, None, None], every_total, 0.0), axis=0
    )
    attended = lax.psum(local_out * jnp.exp(later_sum)[..., None], "kv")
    mean_sq = jnp.mean(attended * attended, axis=2)
    normed = attended * lax.rsqrt(mean_sq + EPS)[..., None]
    normed = (normed.reshape(sequences, head_width) * head_gain).astype(jnp.bfloat16)
    part_out = jnp.dot(normed, w_out, preferred_element_type=jnp.float32)
    return lax.psum(part_out.astype(jnp.bfloat16), "tp")


def solution(mesh):
    return jax.shard_map(
        shards,
        mesh=mesh,
        in_specs=(
            P(None, "kv"),
            P("kv"),
            P("kv", "tp"),
            P("tp"),
            P(None, "kv", "tp"),
            P(None, "kv", "tp"),
            P(),
            P("tp"),
            P("tp", "kv"),
        ),
        out_specs=P(None, "kv"),
        check_vma=False,
    )
```

profile of v0, /device:TPU:0, one launch (start us, length us, event | category | flops | bytes accessed | tf_op | source)
XLA Modules:
  0.0 74.4 jit_solution(1985934041813011728)
XLA Ops:
  0.0 0.0 copy-start
  0.0 0.0 copy-start.4
  0.0 0.0 copy-start.1
  0.0 1.2 %fusion.19 = f32[8,128]{1,0:T(8,128)S(1)} fusion(bf16[256,128]{1,0:T(8,128)(2,1)} %param.11, bf16[8,256]{1,0:T(8,128)(2,1)} %param.9, f32[256]{0:T(256)} %param.10), kind=kOutput, calls=%fused_computation.27 | convolution fusion | flops 530432 | bytes 74752 | tf_op jit(solution)/shard_map/dot_general | solution.py:22
  1.2 0.8 %fusion.18 = f32[8]{0:T(128)S(1)} fusion(bf16[8,256]{1,0:T(8,128)(2,1)} %param.9), kind=kLoop, calls=%fused_computation.26 | loop fusion | flops 6136 | bytes 4128 | tf_op jit(solution)/shard_map/reduce_sum | solution.py:23
  2.0 23.4 %all-reduce.1 = (f32[8,128]{1,0:T(8,128)S(1)}, f32[8]{0:T(128)S(1)}) all-reduce(f32[8,128]{1,0:T(8,128)S(1)} %fusion.19, f32[8]{0:T(128)S(1)} %fusion.18), channel_id=1, replica_groups=mesh['kv'=8,'tp'=4] {'kv'}, use_global_device_ids=true, to_apply=%region_0.0 | all-reduce | flops 1032 | bytes 8256 | tf_op jit(solution)/shard_map/psum | solution.py:24
  25.4 0.1 fusion.25
  25.5 0.0 copy-done
  25.5 0.6 fusion.22
  26.1 0.0 copy-start.2
  26.1 0.0 copy-start.3
  26.8 0.0 copy-done.1
  26.8 0.2 fusion.11
  27.0 0.0 copy-done.4
  27.0 0.7 dynamic-slice
  28.4 0.2 dynamic-update-slice
  28.6 17.1 %all-reduce = f32[64]{0:T(128)S(1)} all-reduce(f32[64]{0:T(128)S(1)} %dynamic-update-slice), channel_id=2, replica_groups=mesh['kv'=8,'tp'=4] {'kv'}, use_global_device_ids=true, to_apply=%add | all-reduce | flops 64 | bytes 512
  45.7 0.1 reshape.93
  45.8 0.1 select_reduce_fusion
  45.9 0.7 fusion.5
  46.7 2.0 %fusion.9 = f32[8,1,128]{2,1,0:T(1,128)S(1)} fusion(bf16[8,1024,128]{2,1,0:T(8,128)(2,1)} %param.14, bf16[8,1024,1]{1,0,2:T(8,128)(2,1)S(1)} %fusion.5), kind=kOutput, calls=%fused_computation.15 | convolution fusion | flops 2097152 | bytes 2117632 | tf_op jit(solution)/shard_map/bhp,bphd->bhd/dot_general | solution.py:44
  48.6 0.1 multiply_bitcast_fusion
  48.7 19.1 %psum.30 = f32[8,1,128]{2,0,1:T(8,128)S(1)} all-reduce(f32[8,1,128]{2,0,1:T(8,128)S(1)} %multiply_bitcast_fusion), channel_id=1, replica_groups=mesh['kv'=8,'tp'=4] {'kv'}, use_global_device_ids=true, to_apply=%region_5.6 | all-reduce | flops 1024 | bytes 8192 | tf_op jit(solution)/shard_map/psum | solution.py:53
  67.8 0.1 multiply_reduce_fusion
  68.0 0.0 copy-done.2
  68.0 0.0 copy-done.3
  68.0 0.2 convolution_convert_fusion
  68.2 6.2 %psum.31 = bf16[8,256]{1,0:T(8,128)(2,1)} all-reduce(bf16[8,256]{1,0:T(8,128)(2,1)S(1)} %convolution_convert_fusion), channel_id=1, replica_groups=mesh['kv'=8,'tp'=4] {'tp'}, use_global_device_ids=true, to_apply=%region_7.8 | all-reduce | flops 2048 | bytes 8192 | tf_op jit(solution)/shard_map/psum | solution.py:58
  (6 shorter events, 0.0 us)
Async XLA Ops:
  0.0 25.5 %copy-start = (bf16[8,1024,128]{2,1,0:T(8,128)(2,1)S(1)}, bf16[8,1024,128]{2,1,0:T(8,128)(2,1)}, u32[]{:S(2)}) copy-start(bf16[8,1024,128]{2,1,0:T(8,128)(2,1)} %param.13) | copy-start | bytes 6291460
  0.0 27.0 %copy-start.4 = (u32[32]{0:T(128)S(1)}, u32[32]{0:T(128)}, u32[]{:S(2)}) copy-start(u32[32]{0:T(128)} %constant.28) | copy-start | bytes 388
  0.0 26.8 %copy-start.1 = (s32[8]{0:T(128)S(1)}, s32[8]{0:T(128)}, u32[]{:S(2)}) copy-start(s32[8]{0:T(128)} %param.15) | copy-start | bytes 100
  26.1 41.9 %copy-start.2 = (bf16[128,256]{1,0:T(8,128)(2,1)S(1)}, bf16[128,256]{1,0:T(8,128)(2,1)}, u32[]{:S(2)}) copy-start(bf16[128,256]{1,0:T(8,128)(2,1)} %param.17) | copy-start | bytes 196612
  26.1 41.9 %copy-start.3 = (f32[128]{0:T(128)S(1)}, f32[128]{0:T(128)}, u32[]{:S(2)}) copy-start(f32[128]{0:T(128)} %param.16) | copy-start | bytes 1540
where the time goes:
time: 74.7 us; the launch traced here: 74.4 us
  blocking collectives  65.9 us (88%)
  matrix products  4.69 us (6%)
  between operations  1.47 us (2%)
  other arithmetic  1.37 us (2%)
  local copies, waits for them, and re-layouts  1.01 us (1%)
    psum x1, blocking collectives, shards(): summed, total_sq = lax.psum((partial_value, squares), 'kv')  23.4 us
    psum x1, blocking collectives, shards(): attended = lax.psum(local_out * jnp.exp(later_sum)[..., None], 'kv')  19.1 us
    unnamed x1, blocking collectives  17.1 us
    psum x1, blocking collectives, shards(): return lax.psum(part_out.astype(jnp.bfloat16), 'tp')  6.23 us
    dot_general x1, matrix products, shards(): jnp.einsum('bhp,bphd->bhd', weights, value_heads, preferred_element_type=...  1.98 us

commit v1 on v0

v1 whole, which is shorter than its diff:
```python
import functools

import jax
import jax.numpy as jnp
from jax import lax
from jax.experimental import pallas as pl
from jax.experimental.pallas import tpu as pltpu
from jax.sharding import PartitionSpec as P

EPS = 1e-06
LANES = 128
MESH = pl.DeviceIdType.MESH


def each(count, body, first=0):
    if count - first <= 16:
        for i in range(first, count):
            body(i)
    else:
        lax.fori_loop(first, count, lambda i, c: (body(i), c)[1], 0)


def folded(count, body, init):
    if count <= 16:
        for i in range(count):
            init = body(i, init)
        return init
    return lax.fori_loop(0, count, body, init)


def push(axis, me, count, buf, send_sem, recv_sem):
    def copy(i):
        return pltpu.make_async_remote_copy(
            src_ref=buf.at[me],
            dst_ref=buf.at[me],
            send_sem=send_sem.at[i],
            recv_sem=recv_sem.at[i],
            device_id={axis: lax.rem(me + i, count)},
            device_id_type=MESH,
        )

    return copy


def arrival(axis, me, count, buf, send_sem, recv_sem):
    def copy(i):
        slot = lax.rem(me + count - i, count)
        return pltpu.make_async_remote_copy(
            src_ref=buf.at[slot],
            dst_ref=buf.at[slot],
            send_sem=send_sem.at[i],
            recv_sem=recv_sem.at[i],
            device_id={axis: slot},
            device_id_type=MESH,
        )

    return copy


def kernel(
    n_kv, n_tp,
    tok_hbm, gain_hbm, wq_hbm, bias_hbm, keys_hbm, values_hbm, len_hbm, hg_hbm, wo_hbm,
    out_ref,
    tok, gain, wq, bias, keys, values, lens, hg, wo,
    qbuf, obuf, tbuf,
    load_sem, key_sem, value_sem,
    q_send, q_recv, o_send, o_recv, t_send, t_recv,
):
    me = lax.axis_index("kv")
    mine = lax.axis_index("tp")
    seqs, local_len, size = keys.shape
    chunks = local_len // LANES

    small = [
        pltpu.make_async_copy(src, dst, load_sem.at[i])
        for i, (src, dst) in enumerate(
            ((tok_hbm, tok), (gain_hbm, gain), (wq_hbm, wq), (bias_hbm, bias),
             (len_hbm, lens), (hg_hbm, hg), (wo_hbm, wo))
        )
    ]
    for copy in small:
        copy.start()
    barrier = pltpu.get_barrier_semaphore()

    def greet(axis, place, count):
        def body(i):
            pl.semaphore_signal(
                barrier, inc=1, device_id={axis: lax.rem(place + i, count)}, device_id_type=MESH
            )

        each(count, body, 1)

    greet("kv", me, n_kv)
    greet("tp", mine, n_tp)
    pairs = seqs // 2
    key_loads = [
        pltpu.make_async_copy(
            keys_hbm.at[pl.ds(2 * i, 2)], keys.at[pl.ds(2 * i, 2)], key_sem.at[i]
        )
        for i in range(pairs)
    ]
    value_loads = [
        pltpu.make_async_copy(
            values_hbm.at[pl.ds(2 * i, 2)], values.at[pl.ds(2 * i, 2)], value_sem.at[i]
        )
        for i in range(pairs)
    ]
    for copy in key_loads + value_loads:
        copy.start()

    for copy in small[:3]:
        copy.wait()
    as_float = tok[...].astype(jnp.float32)
    gained = (as_float * gain[...]).astype(jnp.bfloat16)
    partial = jnp.dot(gained, wq[...], preferred_element_type=jnp.float32)
    squares = jnp.sum(as_float * as_float, axis=1, keepdims=True)
    qbuf[me, pl.ds(0, seqs)] = partial
    qbuf[me, pl.ds(seqs, seqs)] = jnp.broadcast_to(squares, (seqs, size))
    pl.semaphore_wait(barrier, n_kv - 1 + n_tp - 1)
    q_push = push("kv", me, n_kv, qbuf, q_send, q_recv)
    q_arrival = arrival("kv", me, n_kv, qbuf, q_send, q_recv)
    each(n_kv, lambda i: q_push(i).start(), 1)

    for copy in small[3:]:
        copy.wait()
    row = lax.broadcasted_iota(jnp.int32, (seqs, LANES), 0)
    lane = lax.broadcasted_iota(jnp.int32, (seqs, LANES), 1)
    length = jnp.zeros((seqs, LANES), jnp.int32)
    for b in range(seqs):
        length = jnp.where(row == b, lens[b], length)
    left = length - (me * local_len + lane)
    shift = bias[0]
    from_row = lax.broadcasted_iota(jnp.int32, (LANES, 2 * LANES), 0)
    to_lane = lax.broadcasted_iota(jnp.int32, (LANES, 2 * LANES), 1)
    later_of = jnp.where((from_row >= to_lane) | (to_lane >= LANES), 1.0, 0.0).astype(jnp.bfloat16)
    for copy in key_loads:
        copy.wait()

    each(n_kv, lambda i: q_arrival(i).wait_recv(), 1)
    total = folded(n_kv, lambda i, acc: acc + qbuf[i], jnp.zeros((2 * seqs, size), jnp.float32))
    features = tok.shape[1] * n_kv
    row_scale = lax.rsqrt(total[seqs:] / features + EPS)
    queries = total[:seqs] * row_scale
    queries = queries.astype(jnp.bfloat16).astype(jnp.float32)
    qrow = lax.broadcasted_iota(jnp.int32, (seqs, size), 0)

    scores = None
    for i in range(pairs):
        lhs = jnp.concatenate(
            [jnp.where(qrow == 2 * i + k, queries, 0.0) for k in range(2)], axis=1
        ).astype(jnp.bfloat16)
        rhs = jnp.concatenate([keys[2 * i], keys[2 * i + 1]], axis=1)
        term = lax.dot_general(
            lhs, rhs, (((1,), (1,)), ((), ())), preferred_element_type=jnp.float32
        )
        scores = term if scores is None else scores + term
    scores = scores * size ** (-0.5) + shift

    usable, parts = [], []
    for j in range(chunks):
        s = scores[:, j * LANES : (j + 1) * LANES]
        ok = left > j * LANES
        usable.append(ok)
        keep = -(jnp.maximum(s, 0.0) + jnp.log1p(jnp.exp(-jnp.abs(s))))
        parts.append(jnp.where(ok, keep, 0.0))
    keep = jnp.concatenate(parts, axis=0)
    high = keep.astype(jnp.bfloat16)
    rest = keep - high.astype(jnp.float32)
    mid = rest.astype(jnp.bfloat16)
    low = (rest - mid.astype(jnp.float32)).astype(jnp.bfloat16)
    summed = (
        jnp.dot(low, later_of, preferred_element_type=jnp.float32)
        + jnp.dot(mid, later_of, preferred_element_type=jnp.float32)
        + jnp.dot(high, later_of, preferred_element_type=jnp.float32)
    )
    after = jnp.zeros((seqs, LANES), jnp.float32)
    weights = [None] * chunks
    for j in reversed(range(chunks)):
        s = scores[:, j * LANES : (j + 1) * LANES]
        block = summed[j * seqs : (j + 1) * seqs]
        weights[j] = jnp.where(usable[j], jnp.exp(s + (block[:, :LANES] + after)), 0.0)
        after = after + block[:, LANES:]
    weights = jnp.concatenate(weights, axis=1).astype(jnp.bfloat16)

    for copy in value_loads:
        copy.wait()
    local_out = jnp.zeros((seqs, size), jnp.float32)
    for i in range(pairs):
        rhs = jnp.concatenate([values[2 * i], values[2 * i + 1]], axis=1)
        both = jnp.dot(weights, rhs, preferred_element_type=jnp.float32)
        for k in range(2):
            local_out = jnp.where(qrow == 2 * i + k, both[:, k * size : (k + 1) * size], local_out)

    obuf[me, pl.ds(0, seqs)] = local_out
    obuf[me, pl.ds(seqs, seqs)] = after
    o_push = push("kv", me, n_kv, obuf, o_send, o_recv)
    o_arrival = arrival("kv", me, n_kv, obuf, o_send, o_recv)
    each(n_kv, lambda i: o_push(i).start(), 1)
    each(n_kv, lambda i: o_arrival(i).wait_recv(), 1)

    def combine(i, carry):
        attended, later = carry
        slot = n_kv - 1 - i
        got = obuf[slot]
        return attended + jnp.exp(later) * got[:seqs], later + got[seqs:]

    zero = jnp.zeros((seqs, size), jnp.float32)
    attended, _ = folded(n_kv, combine, (zero, zero))
    mean_sq = jnp.mean(attended * attended, axis=1, keepdims=True)
    normed = (attended * lax.rsqrt(mean_sq + EPS) * hg[...]).astype(jnp.bfloat16)
    columns = wo.shape[1]
    part_out = jnp.dot(normed, wo[...], preferred_element_type=jnp.float32).astype(jnp.bfloat16)
    if columns < tbuf.shape[2]:
        tbuf[mine] = jnp.zeros(tbuf.shape[1:], tbuf.dtype)
    tbuf[mine, :, pl.ds(0, columns)] = part_out
    t_push = push("tp", mine, n_tp, tbuf, t_send, t_recv)
    t_arrival = arrival("tp", mine, n_tp, tbuf, t_send, t_recv)
    each(n_tp, lambda i: t_push(i).start(), 1)
    each(n_tp, lambda i: t_arrival(i).wait_recv(), 1)
    mixed = folded(
        n_tp,
        lambda i, acc: acc + tbuf[i].astype(jnp.float32),
        jnp.zeros(tbuf.shape[1:], jnp.float32),
    )
    out_ref[...] = mixed[:, :columns].astype(out_ref.dtype)

    each(n_kv, lambda i: q_push(i).wait_send(), 1)
    each(n_kv, lambda i: o_push(i).wait_send(), 1)
    each(n_tp, lambda i: t_push(i).wait_send(), 1)


def shards(
    n_kv, n_tp,
    tokens, in_gain, w_query, score_bias, cache_keys, cache_values, lengths, head_gain, w_out,
):
    seqs, local_len, size = cache_keys.shape
    assert score_bias.shape[0] == 1 and seqs % 2 == 0 and local_len % LANES == 0
    columns = w_out.shape[1]
    width = -(-columns // LANES) * LANES
    f32, bf16 = jnp.float32, jnp.bfloat16
    any_space = pl.BlockSpec(memory_space=pl.ANY)
    dma = pltpu.SemaphoreType.DMA
    return pl.pallas_call(
        functools.partial(kernel, n_kv, n_tp),
        out_shape=jax.ShapeDtypeStruct((seqs, columns), bf16),
        in_specs=[any_space] * 9,
        out_specs=pl.BlockSpec(memory_space=pltpu.VMEM),
        scratch_shapes=[
            pltpu.VMEM(tokens.shape, bf16),
            pltpu.VMEM((1, in_gain.shape[0]), f32),
            pltpu.VMEM(w_query.shape, bf16),
            pltpu.SMEM(score_bias.shape, f32),
            pltpu.VMEM(cache_keys.shape, bf16),
            pltpu.VMEM(cache_values.shape, bf16),
            pltpu.SMEM(lengths.shape, jnp.int32),
            pltpu.VMEM((1, head_gain.shape[0]), f32),
            pltpu.VMEM(w_out.shape, bf16),
            pltpu.VMEM((n_kv, 2 * seqs, size), f32),
            pltpu.VMEM((n_kv, 2 * seqs, size), f32),
            pltpu.VMEM((n_tp, seqs, width), bf16),
            dma((7,)),
            dma((seqs // 2,)),
            dma((seqs // 2,)),
            dma((n_kv,)),
            dma((n_kv,)),
            dma((n_kv,)),
            dma((n_kv,)),
            dma((n_tp,)),
            dma((n_tp,)),
        ],
        compiler_params=pltpu.CompilerParams(collective_id=0, has_side_effects=True),
    )(
        tokens, in_gain[None], w_query, score_bias, cache_keys, cache_values, lengths,
        head_gain[None], w_out,
    )


def solution(mesh):
    return jax.shard_map(
        functools.partial(shards, mesh.shape["kv"], mesh.shape["tp"]),
        mesh=mesh,
        in_specs=(
            P(None, "kv"),
            P("kv"),
            P("kv", "tp"),
            P("tp"),
            P(None, "kv", "tp"),
            P(None, "kv", "tp"),
            P(),
            P("tp"),
            P("tp", "kv"),
        ),
        out_specs=P(None, "kv"),
        check_vma=False,
    )
```

time: 74.7 us -> 22.3 us (0.30)
  blocking collectives: 65.9 us -> 0 us
  Pallas kernels: 0 us -> 20.1 us
  matrix products: 4.69 us -> 0 us
  other arithmetic: 1.37 us -> 0 us
  between operations: 1.47 us -> 0.66 us
    psum x3 -> x0, blocking collectives: 48.7 us -> none  [the longest x1 23.4 us: shards(): summed, total_sq = lax.psum((partial_value, squares), 'kv')]
    pallas_call x0 -> x1, Pallas kernels: none -> 20.1 us  [shards(): pl.pallas_call(functools.partial(kernel, n_kv, n_tp), out_shape=jax.Shape...]
    unnamed x1 -> x0, blocking collectives: 17.1 us -> none
    dot_general x5 -> x0, matrix products: 4.69 us -> none  [the longest x1 1.98 us: shards(): jnp.einsum('bhp,bphd->bhd', weights, value_heads, preferred_element_type=...]
    reduce_sum x4 -> x0, other arithmetic: 1.2 us -> none  [the longest x1 0.81 us: shards(): squares = jnp.sum(as_float * as_float, axis=1)]
where the time goes in v1:
time: 22.3 us; the launch traced here: 22.1 us
  Pallas kernels  20.1 us (90%)
  local copies, waits for them, and re-layouts  1.28 us (6%)
  between operations  0.66 us (3%)
    pallas_call x1, Pallas kernels, shards(): pl.pallas_call(functools.partial(kernel, n_kv, n_tp), out_shape=jax.Shape...  20.1 us
    unnamed x1, local copies, waits for them, and re-layouts  1.28 us

profile of v1, /device:TPU:0, one launch (start us, length us, event | category | flops | bytes accessed | tf_op | source)
XLA Modules:
  0.0 22.1 jit_solution(5473947390234844622)
XLA Ops:
  0.7 20.1 %shard_map.91 = bf16[8,256]{1,0:T(8,128)(2,1)} custom-call(bf16[8,256]{1,0:T(8,128)(2,1)} %tok_hbm.1, f32[1,256]{1,0:T(1,128)} %bitcast.2, bf16[256,128]{1,0:T(8,128)(2,1)} %wq_hbm.1, f32[1]{0:T(128)S(6)} %copy.11.bias_hbm, bf16[8,1024,128]{2,1,0:T(8,128)(2,1)} %keys_hbm.1, bf16[8,1024,128]{2,1,0:T(8,128)(2,1)} %values_hbm.1, s32[8]{0:T(128)} %len_hbm.1, ...), custom_call_target="tpu_custom_call" | custom-call | tf_op jit(solution)/shard_map/pallas_call | solution.py:243
  20.8 1.3 %copy.12 = bf16[8,256]{1,0:T(8,128)(2,1)} copy(bf16[8,256]{1,0:T(8,128)(2,1)} %shard_map.91) | data formatting | bytes 8192

commit v2 on v1

--- a/solution.py
+++ b/solution.py
@@ -13,7 +13,7 @@
 
 
 def each(count, body, first=0):
-    if count - first <= 16:
+    if count - first <= 32:
         for i in range(first, count):
             body(i)
     else:
@@ -21,18 +21,18 @@
 
 
 def folded(count, body, init):
-    if count <= 16:
+    if count <= 32:
         for i in range(count):
             init = body(i, init)
         return init
     return lax.fori_loop(0, count, body, init)
 
 
-def push(axis, me, count, buf, send_sem, recv_sem):
+def push(axis, me, count, buf, send_sem, recv_sem, part):
     def copy(i):
         return pltpu.make_async_remote_copy(
-            src_ref=buf.at[me],
-            dst_ref=buf.at[me],
+            src_ref=part(buf, me),
+            dst_ref=part(buf, me),
             send_sem=send_sem.at[i],
             recv_sem=recv_sem.at[i],
             device_id={axis: lax.rem(me + i, count)},
@@ -42,15 +42,35 @@
     return copy
 
 
-def arrival(axis, me, count, buf, send_sem, recv_sem):
+def arrival(axis, me, count, buf, send_sem, recv_sem, part):
     def copy(i):
         slot = lax.rem(me + count - i, count)
         return pltpu.make_async_remote_copy(
-            src_ref=buf.at[slot],
-            dst_ref=buf.at[slot],
+            src_ref=part(buf, slot),
+            dst_ref=part(buf, slot),
             send_sem=send_sem.at[i],
             recv_sem=recv_sem.at[i],
             device_id={axis: slot},
+            device_id_type=MESH,
+        )
+
+    return copy
+
+
+def spread(me, mine, n_kv, n_tp, buf, send_sem, recv_sem, rows):
+    def copy(n, arriving):
+        i, k = n % n_kv, n // n_kv
+        if arriving:
+            at, beside = lax.rem(me + n_kv - i, n_kv), lax.rem(mine + n_tp - k, n_tp)
+        else:
+            at, beside = lax.rem(me + i, n_kv), lax.rem(mine + k, n_tp)
+        slot = buf.at[beside, at] if arriving else buf.at[mine, me]
+        return pltpu.make_async_remote_copy(
+            src_ref=slot.at[pl.ds(0, rows)],
+            dst_ref=slot.at[pl.ds(0, rows)],
+            send_sem=send_sem.at[n],
+            recv_sem=recv_sem.at[n],
+            device_id={"kv": at, "tp": beside},
             device_id_type=MESH,
         )
 
@@ -62,9 +82,9 @@
     tok_hbm, gain_hbm, wq_hbm, bias_hbm, keys_hbm, values_hbm, len_hbm, hg_hbm, wo_hbm,
     out_ref,
     tok, gain, wq, bias, keys, values, lens, hg, wo,
-    qbuf, obuf, tbuf,
+    qbuf, obuf,
     load_sem, key_sem, value_sem,
-    q_send, q_recv, o_send, o_recv, t_send, t_recv,
+    q_send, q_recv, o_send, o_recv, w_send, w_recv, h_send, h_recv,
 ):
     me = lax.axis_index("kv")
     mine = lax.axis_index("tp")
@@ -75,7 +95,7 @@
         pltpu.make_async_copy(src, dst, load_sem.at[i])
         for i, (src, dst) in enumerate(
             ((tok_hbm, tok), (gain_hbm, gain), (wq_hbm, wq), (bias_hbm, bias),
-             (len_hbm, lens), (hg_hbm, hg), (wo_hbm, wo))
+             (len_hbm, lens), (hg_hbm, hg.at[mine]), (wo_hbm, wo.at[mine]))
         )
     ]
     for copy in small:
@@ -92,6 +112,7 @@
 
     greet("kv", me, n_kv)
     greet("tp", mine, n_tp)
+    devices = n_kv * n_tp
     pairs = seqs // 2
     key_loads = [
         pltpu.make_async_copy(
@@ -114,17 +135,32 @@
     gained = (as_float * gain[...]).astype(jnp.bfloat16)
     partial = jnp.dot(gained, wq[...], preferred_element_type=jnp.float32)
     squares = jnp.sum(as_float * as_float, axis=1, keepdims=True)
+    row = lax.broadcasted_iota(jnp.int32, (seqs, LANES), 0)
+    lane = lax.broadcasted_iota(jnp.int32, (seqs, LANES), 1)
+    diagonal = row == lane
     qbuf[me, pl.ds(0, seqs)] = partial
-    qbuf[me, pl.ds(seqs, seqs)] = jnp.broadcast_to(squares, (seqs, size))
+    qbuf[me, pl.ds(seqs, 1)] = jnp.sum(jnp.where(diagonal, squares, 0.0), axis=0, keepdims=True)
     pl.semaphore_wait(barrier, n_kv - 1 + n_tp - 1)
-    q_push = push("kv", me, n_kv, qbuf, q_send, q_recv)
-    q_arrival = arrival("kv", me, n_kv, qbuf, q_send, q_recv)
+
+    def q_part(buf, slot):
+        return buf.at[slot, pl.ds(0, seqs + 1)]
+
+    q_push = push("kv", me, n_kv, qbuf, q_send, q_recv, q_part)
+    q_arrival = arrival("kv", me, n_kv, qbuf, q_send, q_recv, q_part)
     each(n_kv, lambda i: q_push(i).start(), 1)
 
     for copy in small[3:]:
         copy.wait()
-    row = lax.broadcasted_iota(jnp.int32, (seqs, LANES), 0)
-    lane = lax.broadcasted_iota(jnp.int32, (seqs, LANES), 1)
+
+    def whole(buf, slot):
+        return buf.at[slot]
+
+    w_push = push("tp", mine, n_tp, wo, w_send, w_recv, whole)
+    w_arrival = arrival("tp", mine, n_tp, wo, w_send, w_recv, whole)
+    h_push = push("tp", mine, n_tp, hg, h_send, h_recv, whole)
+    h_arrival = arrival("tp", mine, n_tp, hg, h_send, h_recv, whole)
+    each(n_tp, lambda i: w_push(i).start(), 1)
+    each(n_tp, lambda i: h_push(i).start(), 1)
     length = jnp.zeros((seqs, LANES), jnp.int32)
     for b in range(seqs):
         length = jnp.where(row == b, lens[b], length)
@@ -137,10 +173,15 @@
         copy.wait()
 
     each(n_kv, lambda i: q_arrival(i).wait_recv(), 1)
-    total = folded(n_kv, lambda i, acc: acc + qbuf[i], jnp.zeros((2 * seqs, size), jnp.float32))
+    total, squares = folded(
+        n_kv,
+        lambda i, acc: (acc[0] + qbuf[i, pl.ds(0, seqs)], acc[1] + qbuf[i, pl.ds(seqs, 1)]),
+        (jnp.zeros((seqs, size), jnp.float32), jnp.zeros((1, size), jnp.float32)),
+    )
+    squares = jnp.sum(jnp.where(diagonal, squares, 0.0), axis=1, keepdims=True)
     features = tok.shape[1] * n_kv
-    row_scale = lax.rsqrt(total[seqs:] / features + EPS)
-    queries = total[:seqs] * row_scale
+    row_scale = lax.rsqrt(squares / features + EPS)
+    queries = total * row_scale
     queries = queries.astype(jnp.bfloat16).astype(jnp.float32)
     qrow = lax.broadcasted_iota(jnp.int32, (seqs, size), 0)
 
@@ -191,42 +232,45 @@
         for k in range(2):
             local_out = jnp.where(qrow == 2 * i + k, both[:, k * size : (k + 1) * size], local_out)
 
-    obuf[me, pl.ds(0, seqs)] = local_out
-    obuf[me, pl.ds(seqs, seqs)] = after
-    o_push = push("kv", me, n_kv, obuf, o_send, o_recv)
-    o_arrival = arrival("kv", me, n_kv, obuf, o_send, o_recv)
-    each(n_kv, lambda i: o_push(i).start(), 1)
-    each(n_kv, lambda i: o_arrival(i).wait_recv(), 1)
-
-    def combine(i, carry):
-        attended, later = carry
-        slot = n_kv - 1 - i
-        got = obuf[slot]
-        return attended + jnp.exp(later) * got[:seqs], later + got[seqs:]
-
-    zero = jnp.zeros((seqs, size), jnp.float32)
-    attended, _ = folded(n_kv, combine, (zero, zero))
-    mean_sq = jnp.mean(attended * attended, axis=1, keepdims=True)
-    normed = (attended * lax.rsqrt(mean_sq + EPS) * hg[...]).astype(jnp.bfloat16)
-    columns = wo.shape[1]
-    part_out = jnp.dot(normed, wo[...], preferred_element_type=jnp.float32).astype(jnp.bfloat16)
-    if columns < tbuf.shape[2]:
-        tbuf[mine] = jnp.zeros(tbuf.shape[1:], tbuf.dtype)
-    tbuf[mine, :, pl.ds(0, columns)] = part_out
-    t_push = push("tp", mine, n_tp, tbuf, t_send, t_recv)
-    t_arrival = arrival("tp", mine, n_tp, tbuf, t_send, t_recv)
-    each(n_tp, lambda i: t_push(i).start(), 1)
-    each(n_tp, lambda i: t_arrival(i).wait_recv(), 1)
-    mixed = folded(
-        n_tp,
-        lambda i, acc: acc + tbuf[i].astype(jnp.float32),
-        jnp.zeros(tbuf.shape[1:], jnp.float32),
-    )
-    out_ref[...] = mixed[:, :columns].astype(out_ref.dtype)
+    after = jnp.sum(jnp.where(diagonal, after, 0.0), axis=0, keepdims=True)
+    first = after.astype(jnp.bfloat16).astype(jnp.float32)
+    second = (after - first).astype(jnp.bfloat16).astype(jnp.float32)
+    third = after - first - second
+    tail = jnp.where(row == 0, first, jnp.where(row == 1, second, jnp.where(row == 2, third, 0.0)))
+    obuf[mine, me] = jnp.concatenate([local_out, tail], axis=0).astype(jnp.bfloat16)
+    spreading = spread(me, mine, n_kv, n_tp, obuf, o_send, o_recv, seqs + 4)
+    each(devices, lambda n: spreading(n, False).start(), 1)
+    each(n_tp, lambda i: w_arrival(i).wait_recv(), 1)
+    each(n_tp, lambda i: h_arrival(i).wait_recv(), 1)
+    each(devices, lambda n: spreading(n, True).wait_recv(), 1)
+
+    mixed = None
+    for t in range(n_tp):
+
+        def combine(i, carry):
+            attended, later = carry
+            slot = n_kv - 1 - i
+            got = obuf[t, slot].astype(jnp.float32)
+            scale = jnp.sum(jnp.where(diagonal, jnp.exp(later), 0.0), axis=1, keepdims=True)
+            later = later + (got[seqs : seqs + 1] + got[seqs + 1 : seqs + 2] + got[seqs + 2 : seqs + 3])
+            return attended + scale * got[:seqs], later
+
+        attended, _ = folded(
+            n_kv,
+            combine,
+            (jnp.zeros((seqs, size), jnp.float32), jnp.zeros((1, LANES), jnp.float32)),
+        )
+        mean_sq = jnp.mean(attended * attended, axis=1, keepdims=True)
+        normed = (attended * lax.rsqrt(mean_sq + EPS) * hg[t]).astype(jnp.bfloat16)
+        part_out = jnp.dot(normed, wo[t], preferred_element_type=jnp.float32)
+        part_out = part_out.astype(jnp.bfloat16).astype(jnp.float32)
+        mixed = part_out if mixed is None else mixed + part_out
+    out_ref[...] = mixed.astype(out_ref.dtype)
 
     each(n_kv, lambda i: q_push(i).wait_send(), 1)
-    each(n_kv, lambda i: o_push(i).wait_send(), 1)
-    each(n_tp, lambda i: t_push(i).wait_send(), 1)
+    each(n_tp, lambda i: w_push(i).wait_send(), 1)
+    each(n_tp, lambda i: h_push(i).wait_send(), 1)
+    each(devices, lambda n: spreading(n, False).wait_send(), 1)
 
 
 def shards(
@@ -236,7 +280,6 @@
     seqs, local_len, size = cache_keys.shape
     assert score_bias.shape[0] == 1 and seqs % 2 == 0 and local_len % LANES == 0
     columns = w_out.shape[1]
-    width = -(-columns // LANES) * LANES
     f32, bf16 = jnp.float32, jnp.bfloat16
     any_space = pl.BlockSpec(memory_space=pl.ANY)
     dma = pltpu.SemaphoreType.DMA
@@ -253,18 +296,19 @@
             pltpu.VMEM(cache_keys.shape, bf16),
             pltpu.VMEM(cache_values.shape, bf16),
             pltpu.SMEM(lengths.shape, jnp.int32),
-            pltpu.VMEM((1, head_gain.shape[0]), f32),
-            pltpu.VMEM(w_out.shape, bf16),
+            pltpu.VMEM((n_tp, 1, size), f32),
+            pltpu.VMEM((n_tp, *w_out.shape), bf16),
             pltpu.VMEM((n_kv, 2 * seqs, size), f32),
-            pltpu.VMEM((n_kv, 2 * seqs, size), f32),
-            pltpu.VMEM((n_tp, seqs, width), bf16),
+            pltpu.VMEM((n_tp, n_kv, 2 * seqs, size), bf16),
             dma((7,)),
             dma((seqs // 2,)),
             dma((seqs // 2,)),
             dma((n_kv,)),
             dma((n_kv,)),
-            dma((n_kv,)),
-            dma((n_kv,)),
+            dma((n_kv * n_tp,)),
+            dma((n_kv * n_tp,)),
+            dma((n_tp,)),
+            dma((n_tp,)),
             dma((n_tp,)),
             dma((n_tp,)),
         ],

time: 22.3 us -> 21 us (0.942)
  Pallas kernels: 20.1 us -> 18.8 us
    pallas_call x1, Pallas kernels: 20.1 us -> 18.8 us  [shards(): pl.pallas_call(functools.partial(kernel, n_kv, n_tp), out_shape=jax.Shape...]
where the time goes in v2:
time: 21 us; the launch traced here: 20.7 us
  Pallas kernels  18.8 us (90%)
  local copies, waits for them, and re-layouts  1.28 us (6%)
  between operations  0.66 us (3%)
    pallas_call x1, Pallas kernels, shards(): pl.pallas_call(functools.partial(kernel, n_kv, n_tp), out_shape=jax.Shape...  18.8 us
    unnamed x1, local copies, waits for them, and re-layouts  1.28 us

profile of v2, /device:TPU:0, one launch (start us, length us, event | category | flops | bytes accessed | tf_op | source)
XLA Modules:
  0.0 20.7 jit_solution(3010469901759175659)
XLA Ops:
  0.7 18.8 %shard_map.91 = bf16[8,256]{1,0:T(8,128)(2,1)} custom-call(bf16[8,256]{1,0:T(8,128)(2,1)} %tok_hbm.1, f32[1,256]{1,0:T(1,128)} %bitcast.2, bf16[256,128]{1,0:T(8,128)(2,1)} %wq_hbm.1, f32[1]{0:T(128)S(6)} %copy.11.bias_hbm, bf16[8,1024,128]{2,1,0:T(8,128)(2,1)} %keys_hbm.1, bf16[8,1024,128]{2,1,0:T(8,128)(2,1)} %values_hbm.1, s32[8]{0:T(128)} %len_hbm.1, ...), custom_call_target="tpu_custom_call" | custom-call | tf_op jit(solution)/shard_map/pallas_call | solution.py:286
  19.5 1.3 %copy.12 = bf16[8,256]{1,0:T(8,128)(2,1)} copy(bf16[8,256]{1,0:T(8,128)(2,1)} %shard_map.91) | data formatting | bytes 8192

commit v3 on v2

--- a/solution.py
+++ b/solution.py
@@ -98,8 +98,6 @@
              (len_hbm, lens), (hg_hbm, hg.at[mine]), (wo_hbm, wo.at[mine]))
         )
     ]
-    for copy in small:
-        copy.start()
     barrier = pltpu.get_barrier_semaphore()
 
     def greet(axis, place, count):
@@ -113,6 +111,8 @@
     greet("kv", me, n_kv)
     greet("tp", mine, n_tp)
     devices = n_kv * n_tp
+    for copy in small:
+        copy.start()
     pairs = seqs // 2
     key_loads = [
         pltpu.make_async_copy(
@@ -147,7 +147,7 @@
 
     q_push = push("kv", me, n_kv, qbuf, q_send, q_recv, q_part)
     q_arrival = arrival("kv", me, n_kv, qbuf, q_send, q_recv, q_part)
-    each(n_kv, lambda i: q_push(i).start(), 1)
+    each(n_kv, lambda i: q_push(n_kv - i).start(), 1)
 
     for copy in small[3:]:
         copy.wait()

time: 21 us -> 20.7 us (0.986)
  Pallas kernels: 18.8 us -> 18.5 us
    pallas_call x1, Pallas kernels: 18.8 us -> 18.5 us  [shards(): pl.pallas_call(functools.partial(kernel, n_kv, n_tp), out_shape=jax.Shape...]
where the time goes in v3:
time: 20.7 us; the launch traced here: 20.5 us
  Pallas kernels  18.5 us (89%)
  local copies, waits for them, and re-layouts  1.28 us (6%)
  between operations  0.66 us (3%)
    pallas_call x1, Pallas kernels, shards(): pl.pallas_call(functools.partial(kernel, n_kv, n_tp), out_shape=jax.Shape...  18.5 us
    unnamed x1, local copies, waits for them, and re-layouts  1.28 us

profile of v3, /device:TPU:0, one launch (start us, length us, event | category | flops | bytes accessed | tf_op | source)
XLA Modules:
  0.0 20.5 jit_solution(6039762258793031772)
XLA Ops:
  0.7 18.5 %shard_map.91 = bf16[8,256]{1,0:T(8,128)(2,1)} custom-call(bf16[8,256]{1,0:T(8,128)(2,1)} %tok_hbm.1, f32[1,256]{1,0:T(1,128)} %bitcast.2, bf16[256,128]{1,0:T(8,128)(2,1)} %wq_hbm.1, f32[1]{0:T(128)S(6)} %copy.11.bias_hbm, bf16[8,1024,128]{2,1,0:T(8,128)(2,1)} %keys_hbm.1, bf16[8,1024,128]{2,1,0:T(8,128)(2,1)} %values_hbm.1, s32[8]{0:T(128)} %len_hbm.1, ...), custom_call_target="tpu_custom_call" | custom-call | tf_op jit(solution)/shard_map/pallas_call | solution.py:286
  19.2 1.3 %copy.12 = bf16[8,256]{1,0:T(8,128)(2,1)} copy(bf16[8,256]{1,0:T(8,128)(2,1)} %shard_map.91) | data formatting | bytes 8192
